TPU v7x, 32 devices: a whole 2x2x4 slice. The times are simulated.
32 devices in a mesh: kv: 16 (over z, y, x), tp: 2 (over core).
Axes of the slice: x: 2, y: 2, z: 4, core: 2. Of those that a mesh axis runs over, the one named last changes fastest.
Arguments:
- tokens: bfloat16 [64, 4096], P(None, 'kv')
- lengths: int32 [16], replicated, may hold values from 1 to 4, 28 in all
- memory: float32 [16, 16, 128, 128], P('kv', 'tp'), may hold values from -0.6 to 0.6
- norm_gain: float32 [4096], P('kv'), may hold values from 0.1 to 1.9
- w_query: bfloat16 [4096, 2048], P('kv', 'tp'), may hold values from -0.09375 to 0.09375
- w_key: bfloat16 [4096, 2048], P('kv', 'tp'), may hold values from -0.09375 to 0.09375
- w_value: bfloat16 [4096, 2048], P('kv', 'tp'), may hold values from -0.09375 to 0.09375
- w_outgate: bfloat16 [4096, 2048], P('kv', 'tp'), may hold values from -0.09375 to 0.09375
- w_alpha: bfloat16 [4096, 16], P('kv'), may hold values from -0.09375 to 0.09375
- w_beta: bfloat16 [4096, 16], P('kv'), may hold values from -0.09375 to 0.09375
- decay_log: float32 [16], P('tp'), may hold values from -4 to 0.5
- decay_bias: float32 [16], P('tp'), may hold values from -1 to 1
- head_gain: float32 [128], replicated, may hold values from 0.1 to 1.9
- w_output: bfloat16 [2048, 4096], P('tp', 'kv'), may hold values from -0.125 to 0.125
- mlp_gain: float32 [4096], P('kv'), may hold values from 0.1 to 1.9
- w_gate: bfloat16 [4096, 11264], P('kv', 'tp'), may hold values from -0.09375 to 0.09375
- w_up: bfloat16 [4096, 11264], P('kv', 'tp'), may hold values from -0.09375 to 0.09375
- w_down: bfloat16 [11264, 4096], P('tp', 'kv'), may hold values from -0.0546875 to 0.0546875
Outputs:
- layer_out: bfloat16 [64, 4096], P(None, 'kv')
- new_memory: float32 [16, 16, 128, 128], P('kv', 'tp')
Inputs may be any that keep to these rules, and one draw needn't show every extreme that they name: How many of a sequence's 4 slots hold live tokens; the live ones come first; the lengths add up to seven quarters of 16, rounded down.
All inputs are finite; a program needn't handle non-finite values.
Results may differ from a plain program's by a relative error of at most 0.012.
Values may be sent and summed in bfloat16 or wider, within the bound.
A program may use at most 64 MiB of HBM per device.

v0:
```python
import jax
import jax.numpy as jnp
from jax import lax
from jax.sharding import PartitionSpec as P

D = 4096
DK = 128
DV = 128
NEW = 4


epsilon = 1e-06


def unit_rows(values):
    return values * lax.rsqrt(jnp.sum(values * values, axis=-1, keepdims=True) + epsilon)


def advance(memory, queries, key_rows, value_rows, decays, betas):
    outputs = []
    for step in range(queries.shape[1]):
        memory = jnp.exp(decays[:, step])[:, :, None, None] * memory
        predicted = jnp.einsum(
            "shde,shd->she", memory, key_rows[:, step], precision=lax.Precision.HIGHEST
        )
        correction = betas[:, step][:, :, None] * (value_rows[:, step] - predicted)
        memory = memory + key_rows[:, step][:, :, :, None] * correction[:, :, None, :]
        outputs.append(
            jnp.einsum("shde,shd->she", memory, queries[:, step], precision=lax.Precision.HIGHEST)
        )
    return (memory, jnp.stack(outputs, axis=1))


def per_device(
    tokens,
    lengths,
    memory,
    norm_gain,
    w_query,
    w_key,
    w_value,
    w_outgate,
    w_alpha,
    w_beta,
    decay_log,
    decay_bias,
    head_gain,
    w_output,
    mlp_gain,
    w_gate,
    w_up,
    w_down,
):
    total_rows = tokens.shape[0]
    kv_count = lax.axis_size("kv")
    kv_place = lax.axis_index("kv")
    tp_place = lax.axis_index("tp")
    own_rows = total_rows // kv_count
    seq_dev = memory.shape[0]
    heads_dev = memory.shape[1]
    token_f = tokens.astype(jnp.float32)
    squares = jnp.sum(token_f * token_f, axis=1)
    scaled = (token_f * norm_gain).astype(jnp.bfloat16)
    part_query = jnp.dot(scaled, w_query, preferred_element_type=jnp.float32)
    part_key = jnp.dot(scaled, w_key, preferred_element_type=jnp.float32)
    part_value = jnp.dot(scaled, w_value, preferred_element_type=jnp.float32)
    part_gate = jnp.dot(scaled, w_outgate, preferred_element_type=jnp.float32)
    part_alpha = jnp.dot(scaled, w_alpha, preferred_element_type=jnp.float32)
    part_beta = jnp.dot(scaled, w_beta, preferred_element_type=jnp.float32)
    all_squares = lax.psum(squares, "kv")
    sum_query, sum_key, sum_value, sum_gate, sum_alpha, sum_beta = (
        lax.psum_scatter(part_query, "kv", scatter_dimension=0, tiled=True),
        lax.psum_scatter(part_key, "kv", scatter_dimension=0, tiled=True),
        lax.psum_scatter(part_value, "kv", scatter_dimension=0, tiled=True),
        lax.psum_scatter(part_gate, "kv", scatter_dimension=0, tiled=True),
        lax.psum_scatter(part_alpha, "kv", scatter_dimension=0, tiled=True),
        lax.psum_scatter(part_beta, "kv", scatter_dimension=0, tiled=True),
    )
    own_squares = lax.dynamic_slice_in_dim(all_squares, kv_place * own_rows, own_rows)
    rstd = lax.rsqrt(own_squares / D + epsilon)[:, None]
    queries = (sum_query * rstd).astype(jnp.bfloat16)
    key_rows = (sum_key * rstd).astype(jnp.bfloat16)
    value_rows = (sum_value * rstd).astype(jnp.bfloat16)
    outgate = (sum_gate * rstd).astype(jnp.bfloat16)
    alphas = lax.dynamic_slice_in_dim(sum_alpha * rstd, tp_place * heads_dev, heads_dev, 1)
    beta_pre = lax.dynamic_slice_in_dim(sum_beta * rstd, tp_place * heads_dev, heads_dev, 1)
    own_lengths = lax.dynamic_slice_in_dim(lengths, kv_place * seq_dev, seq_dev)
    live = jnp.arange(NEW, dtype=jnp.int32)[None, :] < own_lengths[:, None]
    query_h = unit_rows(queries.astype(jnp.float32).reshape(seq_dev, NEW, heads_dev, DK)) * DK ** (
        -0.5
    )
    key_h = unit_rows(key_rows.astype(jnp.float32).reshape(seq_dev, NEW, heads_dev, DK))
    value_h = value_rows.astype(jnp.float32).reshape(seq_dev, NEW, heads_dev, DV)
    decays = -jnp.exp(decay_log) * jax.nn.softplus(alphas + decay_bias)
    decays = jnp.where(live[:, :, None], decays.reshape(seq_dev, NEW, heads_dev), 0.0)
    betas = jnp.where(
        live[:, :, None], jax.nn.sigmoid(beta_pre).reshape(seq_dev, NEW, heads_dev), 0.0
    )
    new_memory, attended = advance(memory, query_h, key_h, value_h, decays, betas)
    attended = attended * lax.rsqrt(jnp.mean(attended * attended, axis=-1, keepdims=True) + epsilon)
    gate_h = outgate.astype(jnp.float32).reshape(seq_dev, NEW, heads_dev, DV)
    mixed = (
        (attended * head_gain * jax.nn.silu(gate_h))
        .astype(jnp.bfloat16)
        .reshape(own_rows, heads_dev * DV)
    )
    attn_terms = jnp.dot(
        lax.all_gather(mixed, "kv", axis=0, tiled=True),
        w_output,
        preferred_element_type=jnp.float32,
    )
    attn_total = lax.psum(attn_terms, "tp")
    hidden = (token_f + attn_total).astype(jnp.bfloat16)
    hidden_f = hidden.astype(jnp.float32)
    hidden_squares = jnp.sum(hidden_f * hidden_f, axis=1)
    hscaled = (hidden_f * mlp_gain).astype(jnp.bfloat16)
    all_live = (jnp.arange(NEW, dtype=jnp.int32)[None, :] < lengths[:, None]).reshape(total_rows)
    part_gate_rows = jnp.dot(hscaled, w_gate, preferred_element_type=jnp.float32)
    part_up_rows = jnp.dot(hscaled, w_up, preferred_element_type=jnp.float32)
    gate_rows, up_rows, mlp_squares = lax.psum((part_gate_rows, part_up_rows, hidden_squares), "kv")
    rstd2 = lax.rsqrt(mlp_squares / D + epsilon)[:, None]
    active = (jax.nn.silu(gate_rows * rstd2) * (up_rows * rstd2)).astype(jnp.bfloat16)
    feed_terms = jnp.dot(active, w_down, preferred_element_type=jnp.float32)
    feed_total = lax.psum(feed_terms.astype(jnp.bfloat16), "tp").astype(jnp.float32)
    layer_out = jnp.where(all_live[:, None], hidden_f + feed_total, 0.0).astype(jnp.bfloat16)
    return (layer_out, new_memory)


def solution(mesh):
    placed = (
        P(None, "kv"),
        P(),
        P("kv", "tp", None, None),
        P("kv"),
        P("kv", "tp"),
        P("kv", "tp"),
        P("kv", "tp"),
        P("kv", "tp"),
        P("kv", None),
        P("kv", None),
        P("tp"),
        P("tp"),
        P(),
        P("tp", "kv"),
        P("kv"),
        P("kv", "tp"),
        P("kv", "tp"),
        P("tp", "kv"),
    )
    return jax.shard_map(
        per_device,
        mesh=mesh,
        in_specs=placed,
        out_specs=(P(None, "kv"), P("kv", "tp", None, None)),
        check_vma=False,
    )
```

profile of v0, /device:TPU:0, one launch (start us, length us, event | category | flops | bytes accessed | tf_op | source)
XLA Modules:
  0.0 358.6 jit_solution(645721127070048668)
XLA Ops:
  7.3 2.1 fusion.61
  9.4 2.0 fusion.63
  11.5 0.9 fusion.65
  12.4 0.9 fusion.69
  13.8 0.6 dynamic_slice.12
  14.4 0.6 iota_compare_fusion.1
  15.0 0.6 dynamic-slice
  16.3 80.4 %all-reduce.6 = (f32[64]{0:T(128)S(1)}, f32[64,16]{1,0:T(8,128)}, f32[64,16]{1,0:T(8,128)}) all-reduce(f32[64]{0:T(128)S(1)} %fusion.38, f32[64,16]{1,0:T(8,128)S(1)} %fusion.71, f32[64,16]{1,0:T(8,128)S(1)} %fusion.67), channel_id=1, replica_groups=mesh['kv'=16,'tp'=2] {'kv'}, use_global_device_ids=true, to_apply=%region_2.0 | all-reduce | flops 2112 | bytes 16896 | tf_op jit(solution)/shard_map/psum | solution.py:70
  96.7 0.8 dynamic-slice_multiply_fusion.4
  97.6 32.9 %all-reduce.17.cloned.1.call-done = (f32[64,1024]{1,0:T(8,128)}, f32[64,1024]{1,0:T(8,128)}, f32[64,1024]{1,0:T(8,128)}, f32[64,1024]{1,0:T(8,128)}) async-done(((f32[64,1024]{1,0:T(8,128)}, f32[64,1024]{1,0:T(8,128)}, f32[64,1024]{1,0:T(8,128)}, f32[64,1024]{1,0:T(8,128)}), (f32[64,1024]{1,0:T(8,128)}, f32[64,1024]{1,0:T(8,128)}, f32[64,1024]{1,0:T(8,128)}, ...) | async-done | bytes 1048592
  130.5 0.9 convert_bitcast_fusion.1
  131.7 0.6 fusion.15
  132.4 0.7 fusion.13
  133.1 0.7 fusion.11
  134.8 0.6 fusion.7
  135.5 0.7 fusion.5
  136.2 0.7 fusion.3
  137.0 0.8 multiply_add_fusion
  137.8 0.8 copy-done.4
  139.3 0.9 fusion.73
  140.2 39.4 %all-gather = bf16[16,4,1024]{2,1,0:T(4,128)(2,1)S(1)} all-gather(bf16[1,4,1024]{2,1,0:T(4,128)(2,1)S(1)} %fusion.73), channel_id=1, replica_groups=mesh['kv'=16,'tp'=2] {'kv'}, dimensions={0}, use_global_device_ids=true | all-gather | bytes 139264 | tf_op jit(solution)/shard_map/all_gather | solution.py:108
  179.6 1.9 fusion.88
  181.5 13.7 %all-reduce.13.cloned.1.call-done = f32[64,256]{1,0:T(8,128)} async-done(((f32[64,256]{1,0:T(8,128)}), f32[64,256]{1,0:T(8,128)}) %all-reduce.13.cloned.1.call-update) | async-done | bytes 65552 | tf_op jit(solution)/shard_map/psum | solution.py:112
  195.2 0.9 fusion.41
  196.2 1.7 fusion.44
  198.0 0.6 copy-done.2
  198.5 1.8 fusion.46
  200.5 43.7 %psum.45 = f32[64]{0:T(128)S(1)} all-reduce(f32[64]{0:T(128)S(1)} %get-tuple-element.11), channel_id=1, replica_groups=mesh['kv'=16,'tp'=2] {'kv'}, use_global_device_ids=true, to_apply=%region_14.15 | all-reduce | flops 64 | bytes 512 | tf_op jit(solution)/shard_map/psum | solution.py:120
  244.2 100.4 %all-reduce.15.cloned.1.call-done = (f32[64,5632]{1,0:T(8,128)}, f32[64,5632]{1,0:T(8,128)}) async-done(((f32[64,5632]{1,0:T(8,128)}, f32[64,5632]{1,0:T(8,128)}), (f32[64,5632]{1,0:T(8,128)}, f32[64,5632]{1,0:T(8,128)})) %all-reduce.15.cloned.1.call-update) | async-done | bytes 2883600 | tf_op jit(solution)/shard_map/psum | solution.py:120
  344.6 3.4 convolution_convert_fusion
  347.9 3.4 psum.47
  351.3 0.7 fusion.43
  (66 shorter events, 3.3 us)
Async XLA Ops:
  7.2 189.0 %copy-start = (bf16[256,5632]{1,0:T(8,128)(2,1)S(1)}, bf16[256,5632]{1,0:T(8,128)(2,1)}, u32[]{:S(2)}) copy-start(bf16[256,5632]{1,0:T(8,128)(2,1)} %param.34) | copy-start | bytes 8650756
  7.2 4.2 %copy-start.3 = (bf16[64,256]{1,0:T(8,128)(2,1)S(1)}, bf16[64,256]{1,0:T(8,128)(2,1)}, u32[]{:S(2)}) copy-start(bf16[64,256]{1,0:T(8,128)(2,1)} %param.18) | copy-start | bytes 98308
  7.2 4.2 %copy-start.7 = (f32[256]{0:T(256)S(1)}, f32[256]{0:T(256)}, u32[]{:S(2)}) copy-start(f32[256]{0:T(256)} %param.21) | copy-start | bytes 3076
  7.2 4.2 %copy-start.5 = (bf16[256,1024]{1,0:T(8,128)(2,1)S(1)}, bf16[256,1024]{1,0:T(8,128)(2,1)}, u32[]{:S(2)}) copy-start(bf16[256,1024]{1,0:T(8,128)(2,1)} %param.24) | copy-start | bytes 1572868
  7.2 123.3 %all-reduce.17.cloned.1.call-start = ((), (), s32[]{:S(2)}) async-start(), calls=%async_computation.2 | async-start | bytes 2097152
  7.3 5.1 %copy-start.6 = (bf16[256,1024]{1,0:T(8,128)(2,1)S(1)}, bf16[256,1024]{1,0:T(8,128)(2,1)}, u32[]{:S(2)}) copy-start(bf16[256,1024]{1,0:T(8,128)(2,1)} %param.23) | copy-start | bytes 1572868
  11.4 2.1 copy-start.8
  11.4 2.2 copy-start.9
  11.4 2.3 copy-start.14
  11.4 2.3 copy-start.13
  11.4 3.6 %copy-start.15 = (u32[32]{0:T(128)S(1)}, u32[32]{0:T(128)}, u32[]{:S(2)}) copy-start(u32[32]{0:T(128)} %constant.45) | copy-start | bytes 388
  11.5 85.3 %copy-start.11 = (f32[128]{0:T(128)S(1)}, f32[128]{0:T(128)}, u32[]{:S(2)}) copy-start(f32[128]{0:T(128)} %param.30) | copy-start | bytes 1540
  11.5 86.0 %copy-start.12 = (f32[8]{0:T(128)S(1)}, f32[8]{0:T(128)}, u32[]{:S(2)}) copy-start(f32[8]{0:T(128)} %param.29) | copy-start | bytes 100
  12.4 119.3 %copy-start.1 = (f32[1,8,128,128]{3,2,1,0:T(8,128)S(1)}, f32[1,8,128,128]{3,2,1,0:T(8,128)}, u32[]{:S(2)}) copy-start(f32[1,8,128,128]{3,2,1,0:T(8,128)} %param.20) | copy-start | bytes 1572868
  13.3 181.9 %all-reduce.13.cloned.1.call-start = ((), (), s32[]{:S(2)}) async-start(), calls=%async_computation | async-start | bytes 131072 | tf_op jit(solution)/shard_map/psum | solution.py:112
  137.0 59.2 %copy-start.10 = (f32[256]{0:T(256)S(1)}, f32[256]{0:T(256)}, u32[]{:S(2)}) copy-start(f32[256]{0:T(256)} %param.32) | copy-start | bytes 3076
  137.8 0.8 copy-start.4
  181.5 163.1 %all-reduce.15.cloned.1.call-start = ((), (), s32[]{:S(2)}) async-start(), calls=%async_computation.1 | async-start | bytes 5767168 | tf_op jit(solution)/shard_map/psum | solution.py:120
  196.2 2.3 copy-start.2
Sparse Core Ops, SparseCore 0:
  14.3 116.1 all-reduce.16
  181.6 13.5 all-reduce.12
  201.0 143.5 all-reduce.14
where the time goes:
time: 359 us
  blocking collectives  167 us (47%)
  waiting for transfers between devices  147 us (41%)
  matrix products  20 us (6%)
  between operations  14.7 us (4%)
  other arithmetic  7.01 us (2%)
    psum x1, waiting for transfers between devices, per_device(): lax.psum((part_gate_rows, part_up_rows, hidden_squares), 'kv')  100 us
    psum x1, blocking collectives, per_device(): all_squares = lax.psum(squares, 'kv')  80.4 us
    psum x1, blocking collectives, per_device(): lax.psum((part_gate_rows, part_up_rows, hidden_squares), 'kv')  43.7 us
    all_gather x1, blocking collectives, per_device(): lax.all_gather(mixed, 'kv', axis=0, tiled=True)  39.4 us
    unnamed x4, waiting for transfers between devices  32.9 us
    psum x1, waiting for transfers between devices, per_device(): attn_total = lax.psum(attn_terms, 'tp')  13.7 us
  transfers between devices with their start and end apart: 3, of which 3 were waited for; matrix products, arithmetic and copies ran while one was open for 1% of the time, Pallas kernels for 0%

commit v1 on v0

--- a/solution.py
+++ b/solution.py
@@ -1,6 +1,8 @@
 import jax
 import jax.numpy as jnp
 from jax import lax
+from jax.experimental import pallas as pl
+from jax.experimental.pallas import tpu as pltpu
 from jax.sharding import PartitionSpec as P
 
 D = 4096
@@ -126,6 +128,541 @@
     return (layer_out, new_memory)
 
 
+F32 = jnp.float32
+BF16 = jnp.bfloat16
+HIGH = lax.Precision.HIGHEST
+TILE = 128
+GROUP = 8
+
+
+def iota(shape, axis):
+    return lax.broadcasted_iota(jnp.int32, shape, axis)
+
+
+def dot(a, b, precision=None):
+    return jnp.dot(a, b, preferred_element_type=F32, precision=precision)
+
+
+def fused(
+    lens,
+    tokens,
+    norm_gain,
+    decay_log,
+    decay_bias,
+    head_gain,
+    mlp_gain,
+    w_alpha,
+    w_beta,
+    memory,
+    w_query,
+    w_key,
+    w_value,
+    w_outgate,
+    w_output,
+    w_gate,
+    w_up,
+    w_down,
+    out,
+    new_memory,
+    v_mem,
+    v_query,
+    v_key,
+    v_value,
+    v_outgate,
+    v_output,
+    v_gate,
+    v_up,
+    v_down,
+    proj_send,
+    proj_recv,
+    rs_buf,
+    xs_buf,
+    kq_buf,
+    r_buf,
+    u_buf,
+    a_buf,
+    ab_buf,
+    mix_buf,
+    mix_all,
+    tp_send,
+    tp_recv,
+    sq_send,
+    sq_recv,
+    gu_send,
+    gu_recv,
+    act_all,
+    load_sem,
+    send_sem,
+    recv_sem,
+    tp_sem,
+):
+    kv_count = mix_all.shape[0]
+    me = lax.axis_index("kv")
+    tp = lax.axis_index("tp")
+    rows, width = tokens.shape
+    heads = v_mem.shape[0]
+    wide = heads * DV
+    compact = tp_send.shape[1]
+    groups = compact // GROUP
+    zones = kv_count // groups
+    chunk = gu_send.shape[2]
+    total_width = width * kv_count
+
+    barrier = pltpu.get_barrier_semaphore()
+
+    @pl.loop(1, kv_count)
+    def _(off):
+        pl.semaphore_signal(
+            barrier,
+            inc=1,
+            device_id={"kv": lax.rem(me + off, kv_count)},
+            device_id_type=pl.DeviceIdType.MESH,
+        )
+
+    pl.semaphore_signal(
+        barrier, inc=1, device_id={"tp": 1 - tp}, device_id_type=pl.DeviceIdType.MESH
+    )
+    pairs = [
+        (w_query, v_query),
+        (w_key, v_key),
+        (w_value, v_value),
+        (w_outgate, v_outgate),
+        (memory, v_mem),
+        (w_output, v_output),
+        (w_gate, v_gate),
+        (w_up, v_up),
+        (w_down, v_down),
+    ]
+    loads = [pltpu.make_async_copy(a, b, load_sem.at[n]) for n, (a, b) in enumerate(pairs)]
+    for load in loads:
+        load.start()
+
+    def remote(src, dst, phase, slot, partner, arrival):
+        return pltpu.make_async_remote_copy(
+            src_ref=src,
+            dst_ref=dst,
+            send_sem=send_sem.at[phase, slot],
+            recv_sem=recv_sem.at[phase, arrival],
+            device_id={"kv": partner},
+            device_id_type=pl.DeviceIdType.MESH,
+        )
+
+    def tp_swap(phase, value):
+        tp_send[phase] = value
+        swap = pltpu.make_async_remote_copy(
+            src_ref=tp_send.at[phase],
+            dst_ref=tp_recv.at[phase],
+            send_sem=tp_sem.at[phase, 0],
+            recv_sem=tp_sem.at[phase, 1],
+            device_id={"tp": 1 - tp},
+            device_id_type=pl.DeviceIdType.MESH,
+        )
+        swap.start()
+        swap.wait()
+        return value + tp_recv[phase]
+
+    all_rows = kv_count * 4 * NEW
+    row = iota((all_rows, rows), 0)
+    spread = jnp.where(
+        iota((all_rows, rows), 1) == (row >> 4) * NEW + (row & 3), 1.0, 0.0
+    ).astype(BF16)
+    tok = tokens[...]
+    scaled = (tok.astype(F32) * norm_gain[...]).astype(BF16)
+    wide_tok = dot(spread, tok)
+    wide_scaled = dot(spread, scaled)
+    squares = jnp.sum(wide_tok * wide_tok, axis=1, keepdims=True)
+    part_of = (iota((all_rows, width), 0) >> 2) & 3
+    all_heads = w_alpha.shape[1]
+    place = iota((all_heads, TILE), 1)
+    head_of = iota((all_heads, TILE), 0)
+    w_small = dot(w_alpha[...], jnp.where(place == head_of, 1.0, 0.0).astype(BF16)) + dot(
+        w_beta[...], jnp.where(place == head_of + all_heads, 1.0, 0.0).astype(BF16)
+    )
+    small = dot(wide_scaled.astype(BF16), w_small.astype(BF16))
+    lane = iota((all_rows, TILE), 1)
+    small = jnp.where(lane == 2 * all_heads, squares, small)
+    part_small = (iota((all_rows, TILE), 0) >> 2) & 3
+    first = small.astype(BF16).astype(F32)
+    second = (small - first).astype(BF16).astype(F32)
+    third = small - first - second
+    pieces = jnp.where(
+        part_small == 0,
+        first,
+        jnp.where(part_small == 1, second, jnp.where(part_small == 2, third, 0.0)),
+    )
+    proj_send[:, :, wide:] = pieces.astype(BF16).reshape(kv_count, 16, TILE)
+    masked = [jnp.where(part_of == p, wide_scaled, 0.0).astype(BF16) for p in range(4)]
+    for load in loads[:4]:
+        load.wait()
+    half = wide // 2
+    for c in range(2):
+        cols = slice(c * half, (c + 1) * half)
+        acc = dot(masked[0], v_query[:, cols])
+        acc = acc + dot(masked[1], v_key[:, cols])
+        acc = acc + dot(masked[2], v_value[:, cols])
+        acc = acc + dot(masked[3], v_outgate[:, cols])
+        proj_send[:, :, cols] = acc.astype(BF16).reshape(kv_count, 16, half)
+
+    pl.semaphore_wait(barrier, kv_count)
+
+    @pl.loop(1, kv_count)
+    def _(off):
+        to = lax.rem(me + off, kv_count)
+        remote(proj_send.at[to], proj_recv.at[me], 0, to, to, me).start()
+
+    slots_wide = kv_count * heads * NEW
+    shape_a = (1, rows)
+    shape_b = (1, slots_wide)
+    shape_c = (rows, compact)
+    length_a = jnp.zeros(shape_a, jnp.int32)
+    start_a = jnp.zeros(shape_a, jnp.int32)
+    length_b = jnp.zeros(shape_b, jnp.int32)
+    start_b = jnp.zeros(shape_b, jnp.int32)
+    length_c = jnp.zeros(shape_c, jnp.int32)
+    start_c = jnp.zeros(shape_c, jnp.int32)
+    seq_a = iota(shape_a, 1) >> 2
+    seq_b = iota(shape_b, 1) >> 5
+    seq_c = iota(shape_c, 0) >> 2
+    begin = jnp.int32(0)
+    for s in range(kv_count):
+        length_a = jnp.where(seq_a == s, lens[s], length_a)
+        start_a = jnp.where(seq_a == s, begin, start_a)
+        length_b = jnp.where(seq_b == s, lens[s], length_b)
+        start_b = jnp.where(seq_b == s, begin, start_b)
+        length_c = jnp.where(seq_c == s, lens[s], length_c)
+        start_c = jnp.where(seq_c == s, begin, start_c)
+        begin = begin + lens[s]
+    slot_a = iota(shape_a, 1) & 3
+    rank_a = jnp.where(slot_a < length_a, start_a + slot_a, -1)
+    pack = jnp.where(rank_a == iota((compact, rows), 0), 1.0, 0.0).astype(BF16)
+    slot_c = iota(shape_c, 0) & 3
+    rank_c = jnp.where(slot_c < length_c, start_c + slot_c, -1)
+    unpack = jnp.where(rank_c == iota(shape_c, 1), 1.0, 0.0).astype(BF16)
+    slot_b = iota(shape_b, 1) & 3
+    head_b = (iota(shape_b, 1) >> 2) & (heads - 1)
+    rank_b = jnp.where(slot_b < length_b, head_b * compact + start_b + slot_b, -1)
+    collect = jnp.where(rank_b == iota((heads * compact, slots_wide), 0), 1.0, 0.0).astype(BF16)
+    tok_packed = dot(pack, tok)
+
+    total = proj_send[me].astype(F32)
+    for off in range(1, kv_count):
+        src = lax.rem(me + off, kv_count)
+        remote(proj_send.at[src], proj_recv.at[src], 0, src, src, src).wait_recv()
+        total = total + proj_recv[src].astype(F32)
+    ab_buf[...] = total[:, wide:]
+    small = ab_buf[0:4, :] + ab_buf[4:8, :] + ab_buf[8:12, :]
+    lane = iota((NEW, TILE), 1)
+    mean_sq = jnp.sum(jnp.where(lane == 2 * all_heads, small, 0.0), axis=1, keepdims=True)
+    rstd = lax.rsqrt(mean_sq / total_width + epsilon)
+    rstd_wide = jnp.broadcast_to(rstd, (NEW, TILE))
+    small = small * rstd
+    ab_buf[0:4, :] = small
+    for p in range(4):
+        rs_buf[p * NEW : (p + 1) * NEW, :] = rstd_wide
+    scale = rs_buf[...]
+    for h in range(heads):
+        piece = total[:, h * DV : (h + 1) * DV] * scale
+        xs_buf[h * 16 : (h + 1) * 16, :] = piece.astype(BF16).astype(F32)
+
+    def slot_rows(ref, index, stride):
+        return ref[pl.ds(index, heads, stride=stride), :]
+
+    query, key_rows, value, gate = (
+        [slot_rows(xs_buf, p * NEW + t, 16) for t in range(NEW)] for p in range(4)
+    )
+    query = [unit_rows(x) * DK ** (-0.5) for x in query]
+    key_rows = [unit_rows(x) for x in key_rows]
+    eye = iota((heads, heads), 0) == iota((heads, heads), 1)
+    rate = jnp.sum(jnp.where(eye, jnp.exp(decay_log[...]), 0.0), axis=1, keepdims=True)
+    bias = jnp.sum(jnp.where(eye, decay_bias[...], 0.0), axis=1, keepdims=True)
+    pick = iota((heads, TILE), 1) - iota((heads, TILE), 0)
+    own_length = jnp.full((heads, 1), lens[me], jnp.int32)
+    decay, beta = [], []
+    for t in range(NEW):
+        line = ab_buf[t : t + 1, :]
+        alpha = jnp.sum(jnp.where(pick == tp * heads, line, 0.0), axis=1, keepdims=True)
+        write = jnp.sum(
+            jnp.where(pick == tp * heads + all_heads, line, 0.0), axis=1, keepdims=True
+        )
+        x = alpha + bias
+        soft = jnp.maximum(x, 0.0) + jnp.log1p(jnp.exp(-jnp.abs(x)))
+        live = own_length > t
+        decay.append(jnp.exp(jnp.where(live, -rate * soft, 0.0)))
+        beta.append(jnp.where(live, jax.nn.sigmoid(write), 0.0))
+    for t in range(NEW):
+        kq_buf[pl.ds(t, heads, stride=8), :] = key_rows[t]
+        kq_buf[pl.ds(NEW + t, heads, stride=8), :] = query[t]
+    loads[4].wait()
+    for h in range(heads):
+        r_buf[h * 8 : (h + 1) * 8, :] = dot(kq_buf[h * 8 : (h + 1) * 8, :], v_mem[h], HIGH)
+    seen_k = [slot_rows(r_buf, t, 8) for t in range(NEW)]
+    seen_q = [slot_rows(r_buf, NEW + t, 8) for t in range(NEW)]
+
+    def inner(a, b):
+        return jnp.sum(a * b, axis=1, keepdims=True)
+
+    corrections = []
+    for t in range(NEW):
+        for r in range(t, NEW):
+            seen_k[r] = seen_k[r] * decay[t]
+            seen_q[r] = seen_q[r] * decay[t]
+        fix = beta[t] * (value[t] - seen_k[t])
+        corrections.append(fix)
+        for r in range(t, NEW):
+            if r > t:
+                seen_k[r] = seen_k[r] + inner(key_rows[t], key_rows[r]) * fix
+            seen_q[r] = seen_q[r] + inner(key_rows[t], query[r]) * fix
+    for t in range(NEW):
+        o = seen_q[t]
+        o = o * lax.rsqrt(jnp.mean(o * o, axis=1, keepdims=True) + epsilon)
+        o = o * head_gain[...] * (gate[t] * jax.nn.sigmoid(gate[t]))
+        mix_buf[pl.ds(t, heads, stride=NEW), :] = o
+    mix_all[me] = mix_buf[...].astype(BF16)
+
+    @pl.loop(1, kv_count)
+    def _(off):
+        to = lax.rem(me + off, kv_count)
+        remote(mix_all.at[me], mix_all.at[me], 1, to, to, me).start()
+
+    u_buf[...] = jnp.zeros_like(u_buf)
+    after = jnp.ones((heads, 1), F32)
+    for t in range(NEW - 1, -1, -1):
+        u_buf[pl.ds(t, heads, stride=8), :] = corrections[t] * after
+        after = after * decay[t]
+    a_buf[...] = jnp.broadcast_to(after, (heads, TILE))
+    for h in range(heads):
+        outer = lax.dot_general(
+            kq_buf[h * 8 : (h + 1) * 8, :],
+            u_buf[h * 8 : (h + 1) * 8, :],
+            (((0,), (0,)), ((), ())),
+            precision=HIGH,
+            preferred_element_type=F32,
+        )
+        v_mem[h] = v_mem[h] * a_buf[h : h + 1, :] + outer
+    store = pltpu.make_async_copy(v_mem, new_memory, load_sem.at[len(pairs)])
+    store.start()
+
+    for off in range(1, kv_count):
+        src = lax.rem(me + off, kv_count)
+        remote(mix_all.at[src], mix_all.at[src], 1, src, src, src).wait_recv()
+    gathered = mix_all[...].reshape(slots_wide, DV)
+    packed = dot(collect, gathered).astype(BF16)
+    loads[5].wait()
+    packed = jnp.concatenate(
+        [packed[h * compact : (h + 1) * compact, :] for h in range(heads)], axis=1
+    )
+    attended = tp_swap(0, dot(packed, v_output[...]))
+    hidden = (tok_packed + attended).astype(BF16).astype(F32)
+    squares = jnp.broadcast_to(
+        jnp.sum(hidden * hidden, axis=1, keepdims=True), (compact, TILE)
+    )
+    sq_send[...] = squares.reshape(groups, GROUP, TILE)
+
+    @pl.loop(1, kv_count)
+    def _(off):
+        to = lax.rem(me + off, kv_count)
+        remote(sq_send.at[lax.rem(to, groups)], sq_recv.at[me], 2, to, to, me).start()
+
+    hscaled = hidden * mlp_gain[...]
+    blank = jnp.zeros((GROUP, width), F32)
+    gate_rows, up_rows = [], []
+    for g in range(groups):
+        own = hscaled[g * GROUP : (g + 1) * GROUP, :]
+        gate_rows += [own, blank]
+        up_rows += [blank, own]
+    gate_rows = jnp.concatenate(gate_rows, axis=0).astype(BF16)
+    up_rows = jnp.concatenate(up_rows, axis=0).astype(BF16)
+    loads[6].wait()
+    loads[7].wait()
+    zone_me = me // groups
+    zone_order = [2, 1, 3, 0] if zones == 4 else list(range(zones))
+    for step in zone_order:
+        zone = lax.rem(zone_me + step, zones)
+        cols = pl.ds(pl.multiple_of(zone * chunk, TILE), chunk)
+        term = dot(gate_rows, v_gate[:, cols]) + dot(up_rows, v_up[:, cols])
+        gu_send[pl.ds(zone * groups, groups)] = term.astype(BF16).reshape(
+            groups, 2 * GROUP, chunk
+        )
+
+        for g in range(groups):
+            if step == 0:
+                if g == 0:
+                    continue
+                to = zone * groups + lax.rem(me + g, groups)
+            else:
+                to = zone * groups + lax.rem(me + g, groups)
+            remote(gu_send.at[to], gu_recv.at[me], 3, to, to, me).start()
+
+    def sources():
+        for step in [0, 1, 3, 2] if zones == 4 else range(zones):
+            for g in range(groups):
+                if step or g:
+                    yield lax.rem(zone_me + step, zones) * groups + lax.rem(me + g, groups)
+
+    mean_sq = sq_send[lax.rem(me, groups)]
+    for src in sources():
+        remote(sq_send.at[0], sq_recv.at[src], 2, src, src, src).wait_recv()
+        mean_sq = mean_sq + sq_recv[src]
+    rstd2 = lax.rsqrt(mean_sq / total_width + epsilon)[:, :1]
+    both = gu_send[me].astype(F32)
+    for src in sources():
+        remote(gu_send.at[src], gu_recv.at[src], 3, src, src, src).wait_recv()
+        both = both + gu_recv[src].astype(F32)
+    gated = both[:GROUP] * rstd2
+    active = gated * jax.nn.sigmoid(gated) * (both[GROUP:] * rstd2)
+    act_all[me] = active.astype(BF16)
+    for step in zone_order:
+        for g in range(groups):
+            if step or g:
+                to = lax.rem(zone_me + step, zones) * groups + lax.rem(me + g, groups)
+                remote(act_all.at[me], act_all.at[me], 4, to, to, me).start()
+    loads[8].wait()
+    feed = jnp.zeros((compact, width), F32)
+    for step in [0, 1, 3, 2] if zones == 4 else range(zones):
+        zone = lax.rem(zone_me + step, zones)
+        for g in range(groups):
+            if step or g:
+                src = zone * groups + lax.rem(me + g, groups)
+                remote(act_all.at[src], act_all.at[src], 4, src, src, src).wait_recv()
+        part = act_all[pl.ds(zone * groups, groups)].astype(F32).reshape(compact, chunk)
+        cols = pl.ds(pl.multiple_of(zone * chunk, TILE), chunk)
+        feed = feed + dot(part.astype(BF16), v_down[cols, :])
+    result = (hidden + tp_swap(1, feed)).astype(BF16)
+    out[...] = dot(unpack, result).astype(BF16)
+
+    store.wait()
+
+    @pl.loop(1, kv_count)
+    def _(off):
+        to = lax.rem(me + off, kv_count)
+        remote(proj_send.at[to], proj_recv.at[me], 0, to, to, me).wait_send()
+        remote(mix_all.at[me], mix_all.at[me], 1, to, to, me).wait_send()
+        remote(sq_send.at[0], sq_recv.at[me], 2, to, to, me).wait_send()
+        remote(gu_send.at[to], gu_recv.at[me], 3, to, to, me).wait_send()
+        remote(act_all.at[me], act_all.at[me], 4, to, to, me).wait_send()
+
+
+def fused_device(
+    tokens,
+    lengths,
+    memory,
+    norm_gain,
+    w_query,
+    w_key,
+    w_value,
+    w_outgate,
+    w_alpha,
+    w_beta,
+    decay_log,
+    decay_bias,
+    head_gain,
+    w_output,
+    mlp_gain,
+    w_gate,
+    w_up,
+    w_down,
+):
+    kv_count = lax.axis_size("kv")
+    rows, width = tokens.shape
+    heads = memory.shape[1]
+    live_rows = (rows // NEW) * 7 // 4
+    compact = -(-live_rows // 16) * 16
+    groups = compact // GROUP
+    zones = kv_count // groups
+    chunk = w_gate.shape[1] // zones
+    wide = heads * DV
+    vmem = pl.BlockSpec(memory_space=pltpu.VMEM)
+    far = pl.BlockSpec(memory_space=pl.ANY)
+    out, state = pl.pallas_call(
+        fused,
+        out_shape=(
+            jax.ShapeDtypeStruct((rows, width), BF16),
+            jax.ShapeDtypeStruct(memory.shape[1:], F32),
+        ),
+        in_specs=[pl.BlockSpec(memory_space=pltpu.SMEM)] + [vmem] * 8 + [far] * 9,
+        out_specs=(vmem, far),
+        scratch_shapes=[
+            pltpu.VMEM(memory.shape[1:], F32),
+            pltpu.VMEM(w_query.shape, BF16),
+            pltpu.VMEM(w_key.shape, BF16),
+            pltpu.VMEM(w_value.shape, BF16),
+            pltpu.VMEM(w_outgate.shape, BF16),
+            pltpu.VMEM(w_output.shape, BF16),
+            pltpu.VMEM(w_gate.shape, BF16),
+            pltpu.VMEM(w_up.shape, BF16),
+            pltpu.VMEM(w_down.shape, BF16),
+            pltpu.VMEM((kv_count, 16, wide + TILE), BF16),
+            pltpu.VMEM((kv_count, 16, wide + TILE), BF16),
+            pltpu.VMEM((16, TILE), F32),
+            pltpu.VMEM((heads * 16, TILE), F32),
+            pltpu.VMEM((heads * 8, TILE), F32),
+            pltpu.VMEM((heads * 8, TILE), F32),
+            pltpu.VMEM((heads * 8, TILE), F32),
+            pltpu.VMEM((heads, TILE), F32),
+            pltpu.VMEM((16, TILE), F32),
+            pltpu.VMEM((heads * NEW, TILE), F32),
+            pltpu.VMEM((kv_count, heads * NEW, TILE), BF16),
+            pltpu.VMEM((2, compact, width), F32),
+            pltpu.VMEM((2, compact, width), F32),
+            pltpu.VMEM((groups, GROUP, TILE), F32),
+            pltpu.VMEM((kv_count, GROUP, TILE), F32),
+            pltpu.VMEM((kv_count, 2 * GROUP, chunk), BF16),
+            pltpu.VMEM((kv_count, 2 * GROUP, chunk), BF16),
+            pltpu.VMEM((kv_count, GROUP, chunk), BF16),
+            pltpu.SemaphoreType.DMA((10,)),
+            pltpu.SemaphoreType.DMA((5, kv_count)),
+            pltpu.SemaphoreType.DMA((5, kv_count)),
+            pltpu.SemaphoreType.DMA((2, 2)),
+        ],
+        compiler_params=pltpu.CompilerParams(
+            collective_id=0, has_side_effects=True, vmem_limit_bytes=48 * 1024 * 1024
+        ),
+    )(
+        lengths,
+        tokens,
+        norm_gain.reshape(1, -1),
+        decay_log.reshape(1, -1),
+        decay_bias.reshape(1, -1),
+        head_gain.reshape(1, -1),
+        mlp_gain.reshape(1, -1),
+        w_alpha,
+        w_beta,
+        memory.reshape(memory.shape[1:]),
+        w_query,
+        w_key,
+        w_value,
+        w_outgate,
+        w_output,
+        w_gate,
+        w_up,
+        w_down,
+    )
+    return out, state.reshape(memory.shape)
+
+
+def fits(tokens, memory, w_gate):
+    kv_count = lax.axis_size("kv")
+    rows, width = tokens.shape
+    live_rows = (rows // NEW) * 7 // 4
+    groups = -(-live_rows // 16) * 16 // GROUP
+    return (
+        lax.axis_size("tp") == 2
+        and memory.shape[0] == 1
+        and memory.shape[1] == 8
+        and rows == kv_count * NEW
+        and rows % 16 == 0
+        and width % TILE == 0
+        and kv_count % groups == 0
+        and w_gate.shape[1] % (kv_count // groups * TILE) == 0
+    )
+
+
+def layer(*arrays):
+    if fits(arrays[0], arrays[2], arrays[15]):
+        return fused_device(*arrays)
+    return per_device(*arrays)
+
+
 def solution(mesh):
     placed = (
         P(None, "kv"),
@@ -148,7 +685,7 @@
         P("tp", "kv"),
     )
     return jax.shard_map(
-        per_device,
+        layer,
         mesh=mesh,
         in_specs=placed,
         out_specs=(P(None, "kv"), P("kv", "tp", None, None)),

time: 359 us -> 79 us (0.22)
  blocking collectives: 167 us -> 0 us
  waiting for transfers between devices: 147 us -> 0 us
  Pallas kernels: 0 us -> 63.7 us
  matrix products: 20 us -> 0 us
  between operations: 14.7 us -> 0.66 us
  local copies, waits for them, and re-layouts: 2.87 us -> 14 us
  other arithmetic: 7.01 us -> 0 us
    psum x3 -> x0, blocking collectives: 127 us -> none  [the longest x1 80.4 us: per_device(): all_squares = lax.psum(squares, 'kv')]
    psum x2 -> x0, waiting for transfers between devices: 114 us -> none  [the longest x1 100 us: per_device(): lax.psum((part_gate_rows, part_up_rows, hidden_squares), 'kv')]
    pallas_call x0 -> x1, Pallas kernels: none -> 63.7 us  [fused_device(): pl.pallas_call(fused, out_shape=(jax.ShapeDtypeStruct((rows, width), BF16...]
    all_gather x1 -> x0, blocking collectives: 39.4 us -> none  [per_device(): lax.all_gather(mixed, 'kv', axis=0, tiled=True)]
    unnamed x4 -> x0, waiting for transfers between devices: 32.9 us -> none
    dot_general x18 -> x0, matrix products: 20 us -> none  [the longest x1 3.35 us: per_device(): feed_terms = jnp.dot(active, w_down, preferred_element_type=jnp.float32)]
    unnamed x35 -> x30, local copies, waits for them, and re-layouts: 2.16 us -> 14 us
  transfers between devices with their start and end apart: 3 -> 0, of which waited for: 3 -> 0; matrix products, arithmetic and copies ran while one was open for 1% -> 0% of each run, Pallas kernels for 0% -> 0%
where the time goes in v1:
time: 79 us; the launch traced here: 78.4 us
  Pallas kernels  63.7 us (81%)
  local copies, waits for them, and re-layouts  14 us (18%)
    pallas_call x1, Pallas kernels, fused_device(): pl.pallas_call(fused, out_shape=(jax.ShapeDtypeStruct((rows, width), BF16...  63.7 us
    unnamed x30, local copies, waits for them, and re-layouts  14 us

profile of v1, /device:TPU:0, one launch (start us, length us, event | category | flops | bytes accessed | tf_op | source)
XLA Modules:
  0.0 78.4 jit_solution(18002440576301090905)
XLA Ops:
  0.6 0.8 %copy.20.w_alpha = bf16[256,16]{1,0:T(8,128)(2,1)S(1)} copy(bf16[256,16]{0,1:T(8,128)(2,1)} %param.26) | data formatting | bytes 16384 | tf_op args[8]
  1.4 0.8 %copy.21.w_beta = bf16[256,16]{1,0:T(8,128)(2,1)S(1)} copy(bf16[256,16]{0,1:T(8,128)(2,1)} %param.27) | data formatting | bytes 16384 | tf_op args[9]
  2.3 0.0 copy-start
  2.3 1.0 %copy-done = f32[1,8,128,128]{3,2,1,0:T(8,128)S(1)} copy-done((f32[1,8,128,128]{3,2,1,0:T(8,128)S(1)}, f32[1,8,128,128]{3,2,1,0:T(8,128)}, u32[]{:S(2)}) %copy-start) | copy-done | bytes 524312
  3.3 0.0 copy-start.1
  3.3 1.0 %copy-done.1 = bf16[256,1024]{1,0:T(8,128)(2,1)S(1)} copy-done((bf16[256,1024]{1,0:T(8,128)(2,1)S(1)}, bf16[256,1024]{1,0:T(8,128)(2,1)}, u32[]{:S(2)}) %copy-start.1) | copy-done | bytes 524312
  4.4 0.0 copy-start.2
  4.4 1.0 %copy-done.2 = bf16[256,1024]{1,0:T(8,128)(2,1)S(1)} copy-done((bf16[256,1024]{1,0:T(8,128)(2,1)S(1)}, bf16[256,1024]{1,0:T(8,128)(2,1)}, u32[]{:S(2)}) %copy-start.2) | copy-done | bytes 524312
  5.4 0.0 copy-start.3
  5.4 1.0 %copy-done.3 = bf16[256,1024]{1,0:T(8,128)(2,1)S(1)} copy-done((bf16[256,1024]{1,0:T(8,128)(2,1)S(1)}, bf16[256,1024]{1,0:T(8,128)(2,1)}, u32[]{:S(2)}) %copy-start.3) | copy-done | bytes 524312
  6.4 0.0 copy-start.4
  6.4 1.0 %copy-done.4 = bf16[256,1024]{1,0:T(8,128)(2,1)S(1)} copy-done((bf16[256,1024]{1,0:T(8,128)(2,1)S(1)}, bf16[256,1024]{1,0:T(8,128)(2,1)}, u32[]{:S(2)}) %copy-start.4) | copy-done | bytes 524312
  7.5 0.0 copy-start.5
  7.5 1.0 %copy-done.5 = bf16[1024,256]{1,0:T(8,128)(2,1)S(1)} copy-done((bf16[1024,256]{1,0:T(8,128)(2,1)S(1)}, bf16[1024,256]{1,0:T(8,128)(2,1)}, u32[]{:S(2)}) %copy-start.5) | copy-done | bytes 524312
  8.5 0.0 copy-start.6
  8.5 0.8 copy-done.6
  9.3 0.0 copy-start.7
  9.3 0.7 copy-done.7
  10.0 0.0 copy-start.8
  10.0 0.7 copy-done.8
  10.6 0.0 copy-start.9
  10.6 0.7 copy-done.9
  11.3 0.0 copy-start.10
  11.3 0.7 copy-done.10
  11.9 0.0 copy-start.11
  12.0 0.7 copy-done.11
  12.6 0.0 copy-start.12
  12.6 0.7 copy-done.12
  13.3 63.7 %shard_map.185 = (bf16[64,256]{1,0:T(8,128)(2,1)S(1)}, f32[8,128,128]{2,1,0:T(8,128)S(1)}) custom-call(s32[16]{0:T(128)S(1)} %copy-done.9, bf16[64,256]{1,0:T(8,128)(2,1)S(1)} %copy-done.6, f32[1,256]{1,0:T(1,128)S(1)} %bitcast.9, f32[1,8]{1,0:T(1,128)S(1)} %bitcast.11, f32[1,8]{1,0:T(1,128)S(1)} %bitcast.12, f32[1,128]{1,0:T(1,128)S(1)} %bitcast.13, ...), custom_call_target="tpu_custom_call" | custom-call | tf_op jit(solution)/shard_map/pallas_call | solution.py:576
  77.0 0.6 copy.24
  77.6 0.8 %copy.25 = f32[1,8,128,128]{3,2,1,0:T(8,128)} copy(f32[1,8,128,128]{3,2,1,0:T(8,128)S(1)} %bitcast.8) | data formatting | bytes 1048576
Async XLA Ops:
  2.3 1.0 %copy-start = (f32[1,8,128,128]{3,2,1,0:T(8,128)S(1)}, f32[1,8,128,128]{3,2,1,0:T(8,128)}, u32[]{:S(2)}) copy-start(f32[1,8,128,128]{3,2,1,0:T(8,128)} %param.20) | copy-start | bytes 1572868
  3.3 1.0 %copy-start.1 = (bf16[256,1024]{1,0:T(8,128)(2,1)S(1)}, bf16[256,1024]{1,0:T(8,128)(2,1)}, u32[]{:S(2)}) copy-start(bf16[256,1024]{1,0:T(8,128)(2,1)} %w_query.1) | copy-start | bytes 1572868
  4.4 1.0 %copy-start.2 = (bf16[256,1024]{1,0:T(8,128)(2,1)S(1)}, bf16[256,1024]{1,0:T(8,128)(2,1)}, u32[]{:S(2)}) copy-start(bf16[256,1024]{1,0:T(8,128)(2,1)} %w_key.1) | copy-start | bytes 1572868
  5.4 1.0 %copy-start.3 = (bf16[256,1024]{1,0:T(8,128)(2,1)S(1)}, bf16[256,1024]{1,0:T(8,128)(2,1)}, u32[]{:S(2)}) copy-start(bf16[256,1024]{1,0:T(8,128)(2,1)} %w_value.1) | copy-start | bytes 1572868
  6.4 1.0 %copy-start.4 = (bf16[256,1024]{1,0:T(8,128)(2,1)S(1)}, bf16[256,1024]{1,0:T(8,128)(2,1)}, u32[]{:S(2)}) copy-start(bf16[256,1024]{1,0:T(8,128)(2,1)} %w_outgate.1) | copy-start | bytes 1572868
  7.5 1.0 %copy-start.5 = (bf16[1024,256]{1,0:T(8,128)(2,1)S(1)}, bf16[1024,256]{1,0:T(8,128)(2,1)}, u32[]{:S(2)}) copy-start(bf16[1024,256]{1,0:T(8,128)(2,1)} %w_output.1) | copy-start | bytes 1572868
  8.5 0.8 copy-start.6
  9.3 0.7 copy-start.7
  10.0 0.7 copy-start.8
  10.6 0.7 copy-start.9
  11.3 0.7 copy-start.10
  11.9 0.7 copy-start.11
  12.6 0.7 copy-start.12

commit v2 on v1

--- a/solution.py
+++ b/solution.py
@@ -175,6 +175,10 @@
     v_down,
     proj_send,
     proj_recv,
+    proj_part,
+    proj_last,
+    small_send,
+    small_recv,
     rs_buf,
     xs_buf,
     kq_buf,
@@ -190,6 +194,8 @@
     sq_recv,
     gu_send,
     gu_recv,
+    gu_part,
+    gu_last,
     act_all,
     load_sem,
     send_sem,
@@ -272,25 +278,21 @@
     wide_scaled = dot(spread, scaled)
     squares = jnp.sum(wide_tok * wide_tok, axis=1, keepdims=True)
     part_of = (iota((all_rows, width), 0) >> 2) & 3
-    all_heads = w_alpha.shape[1]
-    place = iota((all_heads, TILE), 1)
-    head_of = iota((all_heads, TILE), 0)
-    w_small = dot(w_alpha[...], jnp.where(place == head_of, 1.0, 0.0).astype(BF16)) + dot(
-        w_beta[...], jnp.where(place == head_of + all_heads, 1.0, 0.0).astype(BF16)
-    )
-    small = dot(wide_scaled.astype(BF16), w_small.astype(BF16))
+    all_heads = w_alpha.shape[0]
+    place = iota((TILE, all_heads), 0)
+    head_of = iota((TILE, all_heads), 1)
+    w_small = dot(jnp.where(place == head_of, 1.0, 0.0).astype(BF16), w_alpha[...]) + dot(
+        jnp.where(place == head_of + all_heads, 1.0, 0.0).astype(BF16), w_beta[...]
+    )
+    small = lax.dot_general(
+        wide_scaled.astype(BF16),
+        w_small.astype(BF16),
+        (((1,), (1,)), ((), ())),
+        preferred_element_type=F32,
+    )
     lane = iota((all_rows, TILE), 1)
     small = jnp.where(lane == 2 * all_heads, squares, small)
-    part_small = (iota((all_rows, TILE), 0) >> 2) & 3
-    first = small.astype(BF16).astype(F32)
-    second = (small - first).astype(BF16).astype(F32)
-    third = small - first - second
-    pieces = jnp.where(
-        part_small == 0,
-        first,
-        jnp.where(part_small == 1, second, jnp.where(part_small == 2, third, 0.0)),
-    )
-    proj_send[:, :, wide:] = pieces.astype(BF16).reshape(kv_count, 16, TILE)
+    small_send[...] = small.reshape(kv_count, 16, TILE)[:, :GROUP, :]
     masked = [jnp.where(part_of == p, wide_scaled, 0.0).astype(BF16) for p in range(4)]
     for load in loads[:4]:
         load.wait()
@@ -305,10 +307,62 @@
 
     pl.semaphore_wait(barrier, kv_count)
 
+    zone_me = me // groups
+    group_me = lax.rem(me, groups)
+    steps = [2, 1, 3, 0] if zones == 4 else [*range(1, zones), 0]
+
+    def zone_of(step):
+        return lax.rem(zone_me + step, zones)
+
+    def peer(g):
+        return lax.rem(group_me + g, groups)
+
+    def send_plane(send, recv, phase, zone):
+        for g in range(1, groups):
+            slab = zone * groups + peer(g)
+            remote(
+                send.at[slab],
+                recv.at[zone * groups + group_me],
+                phase,
+                slab,
+                zone_me * groups + peer(g),
+                zone * groups + group_me,
+            ).start()
+
+    def sum_plane(send, recv, phase, zone):
+        added = send[zone * groups + group_me].astype(F32)
+        for g in range(1, groups):
+            slab = zone * groups + peer(g)
+            remote(send.at[slab], recv.at[slab], phase, slab, me, slab).wait_recv()
+            added = added + recv[slab].astype(F32)
+        return added
+
+    def reduce_kv(send, recv, part, last, phase):
+        for step in steps[:-1]:
+            zone = zone_of(step)
+            part[zone] = sum_plane(send, recv, phase, zone).astype(BF16)
+            remote(
+                part.at[zone],
+                last.at[zone_me],
+                phase + 1,
+                zone,
+                zone * groups + group_me,
+                zone_me,
+            ).start()
+        added = sum_plane(send, recv, phase, zone_me)
+        for step in steps[:-1][::-1]:
+            zone = zone_of(step)
+            remote(part.at[zone], last.at[zone], phase + 1, zone, me, zone).wait_recv()
+            added = added + last[zone].astype(F32)
+        return added
+
     @pl.loop(1, kv_count)
     def _(off):
         to = lax.rem(me + off, kv_count)
-        remote(proj_send.at[to], proj_recv.at[me], 0, to, to, me).start()
+        remote(small_send.at[to], small_recv.at[me], 5, to, to, me).start()
+
+    for step in steps:
+        send_plane(proj_send, proj_recv, 0, zone_of(step))
 
     slots_wide = kv_count * heads * NEW
     shape_a = (1, rows)
@@ -344,13 +398,13 @@
     collect = jnp.where(rank_b == iota((heads * compact, slots_wide), 0), 1.0, 0.0).astype(BF16)
     tok_packed = dot(pack, tok)
 
-    total = proj_send[me].astype(F32)
+    small = small_send[me]
     for off in range(1, kv_count):
         src = lax.rem(me + off, kv_count)
-        remote(proj_send.at[src], proj_recv.at[src], 0, src, src, src).wait_recv()
-        total = total + proj_recv[src].astype(F32)
-    ab_buf[...] = total[:, wide:]
-    small = ab_buf[0:4, :] + ab_buf[4:8, :] + ab_buf[8:12, :]
+        remote(small_send.at[src], small_recv.at[src], 5, src, src, src).wait_recv()
+        small = small + small_recv[src]
+    small = small[:NEW]
+    total = reduce_kv(proj_send, proj_recv, proj_part, proj_last, 0)
     lane = iota((NEW, TILE), 1)
     mean_sq = jnp.sum(jnp.where(lane == 2 * all_heads, small, 0.0), axis=1, keepdims=True)
     rstd = lax.rsqrt(mean_sq / total_width + epsilon)
@@ -422,7 +476,7 @@
     @pl.loop(1, kv_count)
     def _(off):
         to = lax.rem(me + off, kv_count)
-        remote(mix_all.at[me], mix_all.at[me], 1, to, to, me).start()
+        remote(mix_all.at[me], mix_all.at[me], 2, to, to, me).start()
 
     u_buf[...] = jnp.zeros_like(u_buf)
     after = jnp.ones((heads, 1), F32)
@@ -444,7 +498,7 @@
 
     for off in range(1, kv_count):
         src = lax.rem(me + off, kv_count)
-        remote(mix_all.at[src], mix_all.at[src], 1, src, src, src).wait_recv()
+        remote(mix_all.at[src], mix_all.at[src], 2, src, src, src).wait_recv()
     gathered = mix_all[...].reshape(slots_wide, DV)
     packed = dot(collect, gathered).astype(BF16)
     loads[5].wait()
@@ -461,7 +515,7 @@
     @pl.loop(1, kv_count)
     def _(off):
         to = lax.rem(me + off, kv_count)
-        remote(sq_send.at[lax.rem(to, groups)], sq_recv.at[me], 2, to, to, me).start()
+        remote(sq_send.at[lax.rem(to, groups)], sq_recv.at[me], 6, to, to, me).start()
 
     hscaled = hidden * mlp_gain[...]
     blank = jnp.zeros((GROUP, width), F32)
@@ -474,56 +528,51 @@
     up_rows = jnp.concatenate(up_rows, axis=0).astype(BF16)
     loads[6].wait()
     loads[7].wait()
-    zone_me = me // groups
-    zone_order = [2, 1, 3, 0] if zones == 4 else list(range(zones))
-    for step in zone_order:
-        zone = lax.rem(zone_me + step, zones)
+    for step in steps:
+        zone = zone_of(step)
         cols = pl.ds(pl.multiple_of(zone * chunk, TILE), chunk)
         term = dot(gate_rows, v_gate[:, cols]) + dot(up_rows, v_up[:, cols])
         gu_send[pl.ds(zone * groups, groups)] = term.astype(BF16).reshape(
             groups, 2 * GROUP, chunk
         )
-
-        for g in range(groups):
-            if step == 0:
-                if g == 0:
-                    continue
-                to = zone * groups + lax.rem(me + g, groups)
-            else:
-                to = zone * groups + lax.rem(me + g, groups)
-            remote(gu_send.at[to], gu_recv.at[me], 3, to, to, me).start()
-
-    def sources():
-        for step in [0, 1, 3, 2] if zones == 4 else range(zones):
-            for g in range(groups):
-                if step or g:
-                    yield lax.rem(zone_me + step, zones) * groups + lax.rem(me + g, groups)
-
-    mean_sq = sq_send[lax.rem(me, groups)]
-    for src in sources():
-        remote(sq_send.at[0], sq_recv.at[src], 2, src, src, src).wait_recv()
+        send_plane(gu_send, gu_recv, 3, zone)
+    mean_sq = sq_send[group_me]
+    for off in range(1, kv_count):
+        src = lax.rem(me + off, kv_count)
+        remote(sq_send.at[0], sq_recv.at[src], 6, src, src, src).wait_recv()
         mean_sq = mean_sq + sq_recv[src]
     rstd2 = lax.rsqrt(mean_sq / total_width + epsilon)[:, :1]
-    both = gu_send[me].astype(F32)
-    for src in sources():
-        remote(gu_send.at[src], gu_recv.at[src], 3, src, src, src).wait_recv()
-        both = both + gu_recv[src].astype(F32)
+    both = reduce_kv(gu_send, gu_recv, gu_part, gu_last, 3)
     gated = both[:GROUP] * rstd2
     active = gated * jax.nn.sigmoid(gated) * (both[GROUP:] * rstd2)
     act_all[me] = active.astype(BF16)
-    for step in zone_order:
-        for g in range(groups):
-            if step or g:
-                to = lax.rem(zone_me + step, zones) * groups + lax.rem(me + g, groups)
-                remote(act_all.at[me], act_all.at[me], 4, to, to, me).start()
+
+    def pass_on(zone, slot, partner):
+        block = zone * groups + group_me
+        remote(act_all.at[block], act_all.at[block], 7, slot, partner, block).start()
+
+    def arrive(block):
+        remote(act_all.at[block], act_all.at[block], 7, block, me, block).wait_recv()
+
+    def forward(zone):
+        for g in range(1, groups):
+            pass_on(zone, zone * groups + peer(g), zone_me * groups + peer(g))
+
+    for step in steps[:-1]:
+        there = zone_of(step) * groups + group_me
+        pass_on(zone_me, there, there)
+    forward(zone_me)
+    near_first = [0, 1, 3, 2] if zones == 4 else list(range(zones))
+    for step in near_first[1:]:
+        zone = zone_of(step)
+        arrive(zone * groups + group_me)
+        forward(zone)
     loads[8].wait()
     feed = jnp.zeros((compact, width), F32)
-    for step in [0, 1, 3, 2] if zones == 4 else range(zones):
-        zone = lax.rem(zone_me + step, zones)
-        for g in range(groups):
-            if step or g:
-                src = zone * groups + lax.rem(me + g, groups)
-                remote(act_all.at[src], act_all.at[src], 4, src, src, src).wait_recv()
+    for step in near_first:
+        zone = zone_of(step)
+        for g in range(1, groups):
+            arrive(zone * groups + peer(g))
         part = act_all[pl.ds(zone * groups, groups)].astype(F32).reshape(compact, chunk)
         cols = pl.ds(pl.multiple_of(zone * chunk, TILE), chunk)
         feed = feed + dot(part.astype(BF16), v_down[cols, :])
@@ -535,11 +584,20 @@
     @pl.loop(1, kv_count)
     def _(off):
         to = lax.rem(me + off, kv_count)
-        remote(proj_send.at[to], proj_recv.at[me], 0, to, to, me).wait_send()
-        remote(mix_all.at[me], mix_all.at[me], 1, to, to, me).wait_send()
-        remote(sq_send.at[0], sq_recv.at[me], 2, to, to, me).wait_send()
-        remote(gu_send.at[to], gu_recv.at[me], 3, to, to, me).wait_send()
-        remote(act_all.at[me], act_all.at[me], 4, to, to, me).wait_send()
+        remote(mix_all.at[me], mix_all.at[me], 2, to, to, me).wait_send()
+        remote(small_send.at[to], small_recv.at[me], 5, to, to, me).wait_send()
+        remote(sq_send.at[0], sq_recv.at[me], 6, to, to, me).wait_send()
+        remote(act_all.at[me], act_all.at[me], 7, to, to, me).wait_send()
+
+    for step in steps:
+        zone = zone_of(step)
+        for g in range(1, groups):
+            slab = zone * groups + peer(g)
+            remote(proj_send.at[slab], proj_recv.at[slab], 0, slab, me, slab).wait_send()
+            remote(gu_send.at[slab], gu_recv.at[slab], 3, slab, me, slab).wait_send()
+        if step:
+            remote(proj_part.at[zone], proj_last.at[zone], 1, zone, me, zone).wait_send()
+            remote(gu_part.at[zone], gu_last.at[zone], 4, zone, me, zone).wait_send()
 
 
 def fused_device(
@@ -591,8 +649,12 @@
             pltpu.VMEM(w_gate.shape, BF16),
             pltpu.VMEM(w_up.shape, BF16),
             pltpu.VMEM(w_down.shape, BF16),
-            pltpu.VMEM((kv_count, 16, wide + TILE), BF16),
-            pltpu.VMEM((kv_count, 16, wide + TILE), BF16),
+            pltpu.VMEM((kv_count, 16, wide), BF16),
+            pltpu.VMEM((kv_count, 16, wide), BF16),
+            pltpu.VMEM((zones, 16, wide), BF16),
+            pltpu.VMEM((zones, 16, wide), BF16),
+            pltpu.VMEM((kv_count, GROUP, TILE), F32),
+            pltpu.VMEM((kv_count, GROUP, TILE), F32),
             pltpu.VMEM((16, TILE), F32),
             pltpu.VMEM((heads * 16, TILE), F32),
             pltpu.VMEM((heads * 8, TILE), F32),
@@ -608,14 +670,16 @@
             pltpu.VMEM((kv_count, GROUP, TILE), F32),
             pltpu.VMEM((kv_count, 2 * GROUP, chunk), BF16),
             pltpu.VMEM((kv_count, 2 * GROUP, chunk), BF16),
+            pltpu.VMEM((zones, 2 * GROUP, chunk), BF16),
+            pltpu.VMEM((zones, 2 * GROUP, chunk), BF16),
             pltpu.VMEM((kv_count, GROUP, chunk), BF16),
             pltpu.SemaphoreType.DMA((10,)),
-            pltpu.SemaphoreType.DMA((5, kv_count)),
-            pltpu.SemaphoreType.DMA((5, kv_count)),
+            pltpu.SemaphoreType.DMA((8, kv_count)),
+            pltpu.SemaphoreType.DMA((8, kv_count)),
             pltpu.SemaphoreType.DMA((2, 2)),
         ],
         compiler_params=pltpu.CompilerParams(
-            collective_id=0, has_side_effects=True, vmem_limit_bytes=48 * 1024 * 1024
+            collective_id=0, has_side_effects=True, vmem_limit_bytes=67043328
         ),
     )(
         lengths,
@@ -625,8 +689,8 @@
         decay_bias.reshape(1, -1),
         head_gain.reshape(1, -1),
         mlp_gain.reshape(1, -1),
-        w_alpha,
-        w_beta,
+        w_alpha.T,
+        w_beta.T,
         memory.reshape(memory.shape[1:]),
         w_query,
         w_key,

time: 79 us -> 56.4 us (0.71)
  Pallas kernels: 63.7 us -> 52.2 us
  local copies, waits for them, and re-layouts: 14 us -> 3.25 us
    pallas_call x1, Pallas kernels: 63.7 us -> 52.2 us  [fused_device(): pl.pallas_call(fused, out_shape=(jax.ShapeDtypeStruct((rows, width), BF16...]
    unnamed x30 -> x2, local copies, waits for them, and re-layouts: 14 us -> 3.25 us
where the time goes in v2:
time: 56.4 us; the launch traced here: 56.1 us
  Pallas kernels  52.2 us (93%)
  local copies, waits for them, and re-layouts  3.25 us (6%)
  between operations  0.65 us (1%)
    pallas_call x1, Pallas kernels, fused_device(): pl.pallas_call(fused, out_shape=(jax.ShapeDtypeStruct((rows, width), BF16...  52.2 us
    unnamed x2, local copies, waits for them, and re-layouts  3.25 us

profile of v2, /device:TPU:0, one launch (start us, length us, event | category | flops | bytes accessed | tf_op | source)
XLA Modules:
  0.0 56.1 jit_solution(2185564685483611840)
XLA Ops:
  0.6 52.2 %shard_map.185 = (bf16[64,256]{1,0:T(8,128)(2,1)}, f32[8,128,128]{2,1,0:T(8,128)}) custom-call(s32[16]{0:T(128)} %lens.1, bf16[64,256]{1,0:T(8,128)(2,1)} %tokens.1, f32[1,256]{1,0:T(1,128)} %bitcast.13, f32[1,8]{1,0:T(1,128)} %bitcast.15, f32[1,8]{1,0:T(1,128)} %bitcast.16, f32[1,128]{1,0:T(1,128)} %bitcast.17, f32[1,256]{1,0:T(1,128)} %bitcast.14, ...), custom_call_target="tpu_custom_call" | custom-call | tf_op jit(solution)/shard_map/pallas_call | solution.py:634
  52.8 1.4 %copy.22 = bf16[64,256]{1,0:T(8,128)(2,1)} copy(bf16[64,256]{1,0:T(8,128)(2,1)} %get-tuple-element.8) | data formatting | bytes 65536
  54.2 1.9 %copy.23 = f32[1,8,128,128]{3,2,1,0:T(8,128)} copy(f32[1,8,128,128]{3,2,1,0:T(8,128)} %bitcast.9) | data formatting | bytes 1048576

commit v3 on v2

--- a/solution.py
+++ b/solution.py
@@ -240,7 +240,7 @@
         (w_down, v_down),
     ]
     loads = [pltpu.make_async_copy(a, b, load_sem.at[n]) for n, (a, b) in enumerate(pairs)]
-    for load in loads:
+    for load in loads[:4]:
         load.start()
 
     def remote(src, dst, phase, slot, partner, arrival):
@@ -296,6 +296,8 @@
     masked = [jnp.where(part_of == p, wide_scaled, 0.0).astype(BF16) for p in range(4)]
     for load in loads[:4]:
         load.wait()
+    for load in loads[4:]:
+        load.start()
     half = wide // 2
     for c in range(2):
         cols = slice(c * half, (c + 1) * half)
@@ -309,10 +311,14 @@
 
     zone_me = me // groups
     group_me = lax.rem(me, groups)
-    steps = [2, 1, 3, 0] if zones == 4 else [*range(1, zones), 0]
+    steps = [*range(1, zones), 0]
+    side, odd = zone_me // 2, lax.rem(zone_me, 2)
 
     def zone_of(step):
-        return lax.rem(zone_me + step, zones)
+        if zones != 4:
+            return lax.rem(zone_me + step, zones)
+        across = (1 - side) * 2
+        return [zone_me, across + 1 - odd, across + odd, side * 2 + 1 - odd][step]
 
     def peer(g):
         return lax.rem(group_me + g, groups)
@@ -337,7 +343,7 @@
             added = added + recv[slab].astype(F32)
         return added
 
-    def reduce_kv(send, recv, part, last, phase):
+    def reduce_start(send, recv, part, last, phase):
         for step in steps[:-1]:
             zone = zone_of(step)
             part[zone] = sum_plane(send, recv, phase, zone).astype(BF16)
@@ -349,7 +355,9 @@
                 zone * groups + group_me,
                 zone_me,
             ).start()
-        added = sum_plane(send, recv, phase, zone_me)
+        return sum_plane(send, recv, phase, zone_me)
+
+    def reduce_end(added, part, last, phase):
         for step in steps[:-1][::-1]:
             zone = zone_of(step)
             remote(part.at[zone], last.at[zone], phase + 1, zone, me, zone).wait_recv()
@@ -398,13 +406,13 @@
     collect = jnp.where(rank_b == iota((heads * compact, slots_wide), 0), 1.0, 0.0).astype(BF16)
     tok_packed = dot(pack, tok)
 
+    total = reduce_start(proj_send, proj_recv, proj_part, proj_last, 0)
     small = small_send[me]
     for off in range(1, kv_count):
         src = lax.rem(me + off, kv_count)
         remote(small_send.at[src], small_recv.at[src], 5, src, src, src).wait_recv()
         small = small + small_recv[src]
     small = small[:NEW]
-    total = reduce_kv(proj_send, proj_recv, proj_part, proj_last, 0)
     lane = iota((NEW, TILE), 1)
     mean_sq = jnp.sum(jnp.where(lane == 2 * all_heads, small, 0.0), axis=1, keepdims=True)
     rstd = lax.rsqrt(mean_sq / total_width + epsilon)
@@ -413,19 +421,6 @@
     ab_buf[0:4, :] = small
     for p in range(4):
         rs_buf[p * NEW : (p + 1) * NEW, :] = rstd_wide
-    scale = rs_buf[...]
-    for h in range(heads):
-        piece = total[:, h * DV : (h + 1) * DV] * scale
-        xs_buf[h * 16 : (h + 1) * 16, :] = piece.astype(BF16).astype(F32)
-
-    def slot_rows(ref, index, stride):
-        return ref[pl.ds(index, heads, stride=stride), :]
-
-    query, key_rows, value, gate = (
-        [slot_rows(xs_buf, p * NEW + t, 16) for t in range(NEW)] for p in range(4)
-    )
-    query = [unit_rows(x) * DK ** (-0.5) for x in query]
-    key_rows = [unit_rows(x) for x in key_rows]
     eye = iota((heads, heads), 0) == iota((heads, heads), 1)
     rate = jnp.sum(jnp.where(eye, jnp.exp(decay_log[...]), 0.0), axis=1, keepdims=True)
     bias = jnp.sum(jnp.where(eye, decay_bias[...], 0.0), axis=1, keepdims=True)
@@ -443,6 +438,20 @@
         live = own_length > t
         decay.append(jnp.exp(jnp.where(live, -rate * soft, 0.0)))
         beta.append(jnp.where(live, jax.nn.sigmoid(write), 0.0))
+    total = reduce_end(total, proj_part, proj_last, 0)
+    scale = rs_buf[...]
+    for h in range(heads):
+        piece = total[:, h * DV : (h + 1) * DV] * scale
+        xs_buf[h * 16 : (h + 1) * 16, :] = piece.astype(BF16).astype(F32)
+
+    def slot_rows(ref, index, stride):
+        return ref[pl.ds(index, heads, stride=stride), :]
+
+    query, key_rows, value, gate = (
+        [slot_rows(xs_buf, p * NEW + t, 16) for t in range(NEW)] for p in range(4)
+    )
+    query = [unit_rows(x) * DK ** (-0.5) for x in query]
+    key_rows = [unit_rows(x) for x in key_rows]
     for t in range(NEW):
         kq_buf[pl.ds(t, heads, stride=8), :] = key_rows[t]
         kq_buf[pl.ds(NEW + t, heads, stride=8), :] = query[t]
@@ -536,13 +545,14 @@
             groups, 2 * GROUP, chunk
         )
         send_plane(gu_send, gu_recv, 3, zone)
+    both = reduce_start(gu_send, gu_recv, gu_part, gu_last, 3)
     mean_sq = sq_send[group_me]
     for off in range(1, kv_count):
         src = lax.rem(me + off, kv_count)
         remote(sq_send.at[0], sq_recv.at[src], 6, src, src, src).wait_recv()
         mean_sq = mean_sq + sq_recv[src]
     rstd2 = lax.rsqrt(mean_sq / total_width + epsilon)[:, :1]
-    both = reduce_kv(gu_send, gu_recv, gu_part, gu_last, 3)
+    both = reduce_end(both, gu_part, gu_last, 3)
     gated = both[:GROUP] * rstd2
     active = gated * jax.nn.sigmoid(gated) * (both[GROUP:] * rstd2)
     act_all[me] = active.astype(BF16)
@@ -562,7 +572,7 @@
         there = zone_of(step) * groups + group_me
         pass_on(zone_me, there, there)
     forward(zone_me)
-    near_first = [0, 1, 3, 2] if zones == 4 else list(range(zones))
+    near_first = steps[::-1]
     for step in near_first[1:]:
         zone = zone_of(step)
         arrive(zone * groups + group_me)

time: 56.4 us -> 54.5 us (0.966)
  Pallas kernels: 52.2 us -> 50.3 us
    pallas_call x1, Pallas kernels: 52.2 us -> 50.3 us  [fused_device(): pl.pallas_call(fused, out_shape=(jax.ShapeDtypeStruct((rows, width), BF16...]
where the time goes in v3:
time: 54.5 us; the launch traced here: 54.2 us
  Pallas kernels  50.3 us (92%)
  local copies, waits for them, and re-layouts  3.25 us (6%)
  between operations  0.65 us (1%)
    pallas_call x1, Pallas kernels, fused_device(): pl.pallas_call(fused, out_shape=(jax.ShapeDtypeStruct((rows, width), BF16...  50.3 us
    unnamed x2, local copies, waits for them, and re-layouts  3.25 us

profile of v3, /device:TPU:0, one launch (start us, length us, event | category | flops | bytes accessed | tf_op | source)
XLA Modules:
  0.0 54.2 jit_solution(12248185424427510538)
XLA Ops:
  0.6 50.3 %shard_map.185 = (bf16[64,256]{1,0:T(8,128)(2,1)}, f32[8,128,128]{2,1,0:T(8,128)}) custom-call(s32[16]{0:T(128)} %lens.1, bf16[64,256]{1,0:T(8,128)(2,1)} %tokens.1, f32[1,256]{1,0:T(1,128)} %bitcast.13, f32[1,8]{1,0:T(1,128)} %bitcast.15, f32[1,8]{1,0:T(1,128)} %bitcast.16, f32[1,128]{1,0:T(1,128)} %bitcast.17, f32[1,256]{1,0:T(1,128)} %bitcast.14, ...), custom_call_target="tpu_custom_call" | custom-call | tf_op jit(solution)/shard_map/pallas_call | solution.py:644
  50.9 1.4 %copy.22 = bf16[64,256]{1,0:T(8,128)(2,1)} copy(bf16[64,256]{1,0:T(8,128)(2,1)} %get-tuple-element.8) | data formatting | bytes 65536
  52.3 1.9 %copy.23 = f32[1,8,128,128]{3,2,1,0:T(8,128)} copy(f32[1,8,128,128]{3,2,1,0:T(8,128)} %bitcast.9) | data formatting | bytes 1048576
